TPU v7x, 32 devices: a whole 2x2x4 slice. The times are simulated.
32 devices in a mesh: grp: 2 (over y), fs: 4 (over z), tp: 4 (over x, core).
Axes of the slice: x: 2, y: 2, z: 4, core: 2. Of those that a mesh axis runs over, the one named last changes fastest.
Arguments:
- tokens: bfloat16 [3072, 2048], P(('grp', 'fs')), parts along dimension 0, may hold values from -3 to 3
- gate_weight: bfloat16 [2048, 5120], P('fs', 'tp'), may hold values from -0.125 to 0.125
- up_weight: bfloat16 [2048, 5120], P('fs', 'tp'), may hold values from -0.125 to 0.125
- down_weight: bfloat16 [5120, 2048], P('tp', 'fs'), may hold values from -0.078125 to 0.078125
- pool_weight: bfloat16 [512, 4, 512], P('fs', None, 'tp'), may hold values from -0.375 to 0.375
- pool_bias: float32 [4, 512], replicated, may hold values from -3 to 3
- pool_scale: float32 [2048], replicated, may hold values from 0.1 to 1.9
- gain_first: float32 [2048], replicated, may hold values from 0.1 to 1.9
- gain_mix: float32 [2048], replicated, may hold values from 0.1 to 1.9
- gain_second: float32 [2048], replicated, may hold values from 0.1 to 1.9
Outputs:
- result: bfloat16 [3072, 2048], P(('grp', 'fs')), parts along dimension 0
There are 2 independent parts, one for each index of `grp`. A program takes and returns all parts, laid end to end along the dimension named above; an argument that names none is the same for every part. Nothing has to cross between parts.
All inputs are finite; a program needn't handle non-finite values.
Results may differ from a plain program's by a relative error of at most 0.018.
Values may be sent and summed in bfloat16 or wider, within the bound.
A program may use at most 64 MiB of HBM per device.

v0:
```python
import jax
import jax.numpy as jnp
from jax import lax
from jax.sharding import PartitionSpec as P

eps = 1e-06
pool_spans = (2, 4, 8, 16)
pad_width = 8


def rms_scale(values, gain_vec):
    fvalues = values.astype(jnp.float32)
    scaled = fvalues * lax.rsqrt(jnp.mean(fvalues * fvalues, axis=-1, keepdims=True) + eps)
    return (scaled * gain_vec).astype(jnp.bfloat16)


def ffn_hidden(normed, gate_full, up_full):
    gate_proj = jnp.dot(normed, gate_full, preferred_element_type=jnp.float32)
    up_proj = jnp.dot(normed, up_full, preferred_element_type=jnp.float32)
    return (jax.nn.silu(gate_proj) * up_proj).astype(jnp.bfloat16)


def pool_block(padded, offset, seq_len, pool_full, pool_bias, pool_scale):
    n_tokens = padded.shape[0] - 2 * pad_width
    group_width = pool_full.shape[0]
    position = offset + lax.iota(jnp.int32, n_tokens)
    column_pos = offset - pad_width + lax.iota(jnp.int32, padded.shape[0])
    center = padded[pad_width : pad_width + n_tokens].astype(jnp.float32)
    outputs = []
    for group_number, window_span in enumerate(pool_spans):
        low_edge = jnp.clip(position - window_span // 2, 0, seq_len)
        high_edge = jnp.clip(position - window_span // 2 + window_span, 0, seq_len)
        band_mask = (
            (column_pos[None, :] >= low_edge[:, None]) & (column_pos[None, :] < high_edge[:, None])
        ).astype(jnp.bfloat16)
        lower_col = group_number * group_width
        columns = padded[:, lower_col : lower_col + group_width]
        window_sum = jnp.dot(band_mask, columns, preferred_element_type=jnp.float32)
        window_mean = window_sum / (high_edge - low_edge).astype(jnp.float32)[:, None]
        deviation = (window_mean - center[:, lower_col : lower_col + group_width]).astype(
            jnp.bfloat16
        )
        mapped = jnp.dot(
            deviation, pool_full[:, group_number, :], preferred_element_type=jnp.float32
        )
        outputs.append(mapped + pool_bias[group_number])
    return jnp.concatenate(outputs, axis=-1) * pool_scale


def shards(
    tokens,
    gate_weight,
    up_weight,
    down_weight,
    pool_weight,
    pool_bias,
    pool_scale,
    gain_first,
    gain_mix,
    gain_second,
):
    gate_full, up_full, pool_half = (
        lax.all_gather(gate_weight, "fs", axis=0, tiled=True),
        lax.all_gather(up_weight, "fs", axis=0, tiled=True),
        lax.all_gather(pool_weight, "fs", axis=0, tiled=True),
    )
    down_full = lax.all_gather(down_weight, "fs", axis=1, tiled=True)
    pool_full = lax.all_gather(pool_half, "tp", axis=2, tiled=True)
    seq_len = tokens.shape[0]
    first_normed = rms_scale(tokens, gain_first)
    first_hidden = ffn_hidden(first_normed, gate_full, up_full)
    second_gate, second_up, second_down = (gate_full, up_full, down_full)
    first_branch = lax.psum(
        jnp.dot(first_hidden, down_full, preferred_element_type=jnp.float32).astype(jnp.bfloat16),
        "tp",
    ).astype(jnp.float32)
    after_first = (tokens.astype(jnp.float32) + 0.5 * first_branch).astype(jnp.bfloat16)
    mix_normed = rms_scale(after_first, gain_mix)
    padded = jnp.pad(mix_normed, ((pad_width, pad_width), (0, 0)))
    mixed = pool_block(padded, 0, seq_len, pool_full, pool_bias, pool_scale)
    after_mix = (after_first.astype(jnp.float32) + mixed).astype(jnp.bfloat16)
    second_normed = rms_scale(after_mix, gain_second)
    second_hidden = ffn_hidden(second_normed, second_gate, second_up)
    second_branch = lax.psum(
        jnp.dot(second_hidden, second_down, preferred_element_type=jnp.float32).astype(
            jnp.bfloat16
        ),
        "tp",
    ).astype(jnp.float32)
    return (after_mix.astype(jnp.float32) + 0.5 * second_branch).astype(jnp.bfloat16)


def solution(mesh):
    return jax.shard_map(
        shards,
        mesh=mesh,
        in_specs=(
            P(("grp", "fs"), None),
            P("fs", "tp"),
            P("fs", "tp"),
            P("tp", "fs"),
            P("fs", None, "tp"),
            P(),
            P(),
            P(),
            P(),
            P(),
        ),
        out_specs=P(("grp", "fs"), None),
        check_vma=False,
    )
```

profile of v0, /device:TPU:0, one launch (start us, length us, event | category | flops | bytes accessed | tf_op | source)
XLA Modules:
  0.0 468.3 jit_solution(4957366809883981244)
XLA Ops:
  6.5 0.7 all-gather.5.cloned.1.call-update
  7.3 0.7 all-gather.7.cloned.1.call-update
  8.1 0.7 all-gather.9.cloned.1.call-update
  8.8 0.4 fusion
  9.2 100.5 %all-gather.5.cloned.1.call-done = bf16[2048,1280]{1,0:T(8,128)(2,1)} async-done(((bf16[512,1280]{1,0:T(8,128)(2,1)}), bf16[2048,1280]{1,0:T(8,128)(2,1)}) %all-gather.5.cloned.1.call-update) | async-done | bytes 5242896 | tf_op jit(solution)/shard_map/all_gather | solution.py:63
  109.7 6.0 %fusion.56 = f32[384,1280]{1,0:T(8,128)} fusion(bf16[2048,1280]{1,0:T(8,128)(2,1)} %all-gather.5.cloned.1.call-done, bf16[384,2048]{1,0:T(8,128)(2,1)S(1)} %copy-done, f32[2048]{0:T(1024)S(1)} %copy-done.8, f32[384]{0:T(512)S(1)} %add_rsqrt_fusion.2), kind=kOutput, calls=%fused_computation.69 | convolution fusion | flops 2016411648 | bytes 8791552 | tf_op jit(solution)/shard_map/dot_general | solution.py:18
  115.7 92.0 %all-gather.7.cloned.1.call-done = bf16[2048,1280]{1,0:T(8,128)(2,1)} async-done(((bf16[512,1280]{1,0:T(8,128)(2,1)}), bf16[2048,1280]{1,0:T(8,128)(2,1)}) %all-gather.7.cloned.1.call-update) | async-done | bytes 5242896 | tf_op jit(solution)/shard_map/all_gather | solution.py:64
  207.7 98.0 %all-gather.9.cloned.1.call-done = bf16[1280,2048]{1,0:T(8,128)(2,1)} async-done(((bf16[1280,512]{1,0:T(8,128)(2,1)}), bf16[1280,2048]{1,0:T(8,128)(2,1)}) %all-gather.9.cloned.1.call-update) | async-done | bytes 5242896 | tf_op jit(solution)/shard_map/all_gather | solution.py:67
  305.6 10.6 %convolution_convert_fusion.1 = bf16[384,2048]{1,0:T(8,128)(2,1)} fusion(bf16[1280,2048]{1,0:T(8,128)(2,1)} %all-gather.9.cloned.1.call-done, bf16[2048,1280]{1,0:T(8,128)(2,1)} %all-gather.7.cloned.1.call-done, f32[384,1280]{1,0:T(8,128)} %fusion.56, bf16[384,2048]{1,0:T(8,128)(2,1)S(1)} %copy-done, f32[2048]{0:T(1024)S(1)} %copy-done.8, ...), kind=kOutput, calls=%fused_computation.25 | convolution fusion | flops 4033413120 | bytes 15607296 | tf_op jit(solution)/shard_map/dot_general | solution.py:74
  316.4 16.7 %all_gather.18 = bf16[512,4,128]{2,0,1:T(8,128)(2,1)} all-gather(bf16[128,4,128]{2,0,1:T(8,128)(2,1)S(1)} %copy.11), channel_id=1, replica_groups=mesh['grp'=2,'fs'=4,'tp'=4] {'fs'}, dimensions={0}, use_global_device_ids=true | all-gather | bytes 655360 | tf_op jit(solution)/shard_map/all_gather | solution.py:65
  333.4 24.2 %all-reduce.4.cloned.1.call-done = bf16[384,2048]{1,0:T(8,128)(2,1)} async-done(((bf16[384,2048]{1,0:T(8,128)(2,1)}), bf16[384,2048]{1,0:T(8,128)(2,1)}) %all-reduce.4.cloned.1.call-update) | async-done | bytes 1572880 | tf_op jit(solution)/shard_map/psum | solution.py:73
  357.7 2.2 fusion.4
  359.9 3.0 fusion.97
  362.9 19.0 %all-gather.11.cloned.1.call-done = bf16[512,4,512]{2,0,1:T(8,128)(2,1)} async-done(((bf16[512,4,128]{2,0,1:T(8,128)(2,1)}), bf16[512,4,512]{2,0,1:T(8,128)(2,1)}) %all-gather.11.cloned.1.call-update) | async-done | bytes 2097168 | tf_op jit(solution)/shard_map/all_gather | solution.py:68
  382.0 3.0 convolution_add_fusion
  384.9 3.0 convolution_add_fusion.1
  387.9 3.0 convolution_add_fusion.2
  390.9 3.0 convolution_add_fusion.3
  393.9 2.9 fusion.8
  396.8 1.1 copy-done.2
  398.0 6.0 %fusion.52 = f32[384,1280]{1,0:T(8,128)} fusion(bf16[2048,1280]{1,0:T(8,128)(2,1)} %all-gather.5.cloned.1.call-done, bf16[384,2048]{1,0:T(8,128)(2,1)S(1)} %get-tuple-element.6, f32[2048]{0:T(1024)S(1)} %copy-done.9, f32[384]{0:T(512)S(1)} %add_rsqrt_fusion), kind=kOutput, calls=%fused_computation.68 | convolution fusion | flops 2016411648 | bytes 8791552 | tf_op jit(solution)/shard_map/dot_general | solution.py:18
  404.0 11.2 %convolution_convert_fusion = bf16[384,2048]{1,0:T(8,128)(2,1)} fusion(bf16[1280,2048]{1,0:T(8,128)(2,1)} %all-gather.9.cloned.1.call-done, bf16[2048,1280]{1,0:T(8,128)(2,1)} %all-gather.7.cloned.1.call-done, f32[384,1280]{1,0:T(8,128)} %fusion.52, bf16[384,2048]{1,0:T(8,128)(2,1)} %copy-done.2, f32[2048]{0:T(1024)S(1)} %copy-done.9, f32[384]{0:T(512)S(1)} %add_rsqrt_fusion), kind=kOutput, calls=%fused_computation.24 | convolution fusion | flops 4033413120 | bytes 15607296 | tf_op jit(solution)/shard_map/dot_general | solution.py:85
  415.2 43.0 %all-reduce.6.cloned.1.call-done = bf16[384,2048]{1,0:T(8,128)(2,1)} async-done(((bf16[384,2048]{1,0:T(8,128)(2,1)}), bf16[384,2048]{1,0:T(8,128)(2,1)}) %all-reduce.6.cloned.1.call-update) | async-done | bytes 1572880 | tf_op jit(solution)/shard_map/psum | solution.py:84
  458.2 3.2 fusion.11
  (42 shorter events, 0.6 us)
Async XLA Ops:
  6.5 2.3 copy-start
  6.5 103.2 %copy-start.8 = (f32[2048]{0:T(1024)S(1)}, f32[2048]{0:T(1024)}, u32[]{:S(2)}) copy-start(f32[2048]{0:T(1024)} %param.17) | copy-start | bytes 24580
  6.5 103.2 %all-gather.5.cloned.1.call-start = ((), (), s32[]{:S(2)}) async-start(), calls=%async_computation | async-start | bytes 6553600 | tf_op jit(solution)/shard_map/all_gather | solution.py:63
  7.3 200.4 %all-gather.7.cloned.1.call-start = ((), (), s32[]{:S(2)}) async-start(), calls=%async_computation.1 | async-start | bytes 6553600 | tf_op jit(solution)/shard_map/all_gather | solution.py:64
  8.0 297.6 %all-gather.9.cloned.1.call-start = ((), (), s32[]{:S(2)}) async-start(), calls=%async_computation.2 | async-start | bytes 6553600 | tf_op jit(solution)/shard_map/all_gather | solution.py:67
  8.7 348.9 %all-reduce.4.cloned.1.call-start = ((), (), s32[]{:S(2)}) async-start(), calls=%async_computation.3 | async-start | bytes 3145728 | tf_op jit(solution)/shard_map/psum | solution.py:73
  115.7 200.7 %copy-start.4 = (bf16[128,4,128]{2,1,0:T(4,128)(2,1)S(1)}, bf16[128,4,128]{2,1,0:T(4,128)(2,1)}, u32[]{:S(2)}) copy-start(bf16[128,4,128]{2,1,0:T(4,128)(2,1)} %param.14) | copy-start | bytes 393220
  115.7 217.7 %copy-start.7 = (f32[4,512]{1,0:T(4,128)S(1)}, f32[4,512]{1,0:T(4,128)}, u32[]{:S(2)}) copy-start(f32[4,512]{1,0:T(4,128)} %param.15) | copy-start | bytes 24580
  316.3 43.6 %copy-start.5 = (f32[2048]{0:T(1024)S(1)}, f32[2048]{0:T(1024)}, u32[]{:S(2)}) copy-start(f32[2048]{0:T(1024)} %param.18) | copy-start | bytes 24580
  316.3 65.6 %all-gather.11.cloned.1.call-start = ((), (), s32[]{:S(2)}) async-start(), calls=%async_computation.4 | async-start | bytes 2621440 | tf_op jit(solution)/shard_map/all_gather | solution.py:68
  333.1 125.1 %all-reduce.6.cloned.1.call-start = ((), (), s32[]{:S(2)}) async-start(), calls=%async_computation.5 | async-start | bytes 3145728 | tf_op jit(solution)/shard_map/psum | solution.py:84
  357.6 2.2 copy-start.1
  390.9 3.0 copy-start.6
  393.9 4.1 copy-start.9
  396.8 1.1 copy-start.2
  404.0 54.2 %copy-start.3 = (bf16[384,2048]{1,0:T(8,128)(2,1)S(1)}, bf16[384,2048]{1,0:T(8,128)(2,1)}, u32[]{:S(2)}) copy-start(bf16[384,2048]{1,0:T(8,128)(2,1)} %copy-done.2) | copy-start | bytes 4718596
Sparse Core Ops, SparseCore 0:
  8.9 100.7 all-gather.4
  111.3 96.3 all-gather.6
  209.2 96.3 all-gather.8
  316.4 41.1 all-reduce.3
  359.0 22.8 all-gather.10
  415.3 42.8 all-reduce.5
where the time goes:
time: 469 us; the launch traced here: 468 us
  waiting for transfers between devices  379 us (81%)
  matrix products  45.8 us (10%)
  blocking collectives  16.7 us (4%)
  between operations  13.6 us (3%)
  other arithmetic  11.8 us (3%)
    all_gather x1, waiting for transfers between devices, shards(): lax.all_gather(gate_weight, 'fs', axis=0, tiled=True)  101 us
    all_gather x1, waiting for transfers between devices, shards(): down_full = lax.all_gather(down_weight, 'fs', axis=1, tiled=True)  98 us
    all_gather x1, waiting for transfers between devices, shards(): lax.all_gather(up_weight, 'fs', axis=0, tiled=True)  92 us
    psum x1, waiting for transfers between devices, shards(): lax.psum(jnp.dot(second_hidden, second_down, preferred_element_type=jnp.f...  43 us
    psum x1, waiting for transfers between devices, shards(): lax.psum(jnp.dot(first_hidden, down_full, preferred_element_type=jnp.floa...  24.2 us
    all_gather x1, waiting for transfers between devices, shards(): pool_full = lax.all_gather(pool_half, 'tp', axis=2, tiled=True)  19 us
    all_gather x1, blocking collectives, shards(): lax.all_gather(pool_weight, 'fs', axis=0, tiled=True)  16.7 us
    dot_general x2, matrix products, ffn_hidden(): gate_proj = jnp.dot(normed, gate_full, preferred_element_type=jnp.float32)  12 us
  transfers between devices with their start and end apart: 6, of which 6 were waited for; matrix products, arithmetic and copies ran while one was open for 3% of the time, Pallas kernels for 0%

commit v1 on v0

--- a/solution.py
+++ b/solution.py
@@ -6,6 +6,11 @@
 eps = 1e-06
 pool_spans = (2, 4, 8, 16)
 pad_width = 8
+
+
+def swapped_in(x, axis, dim):
+    sent = jnp.stack([x] * lax.axis_size(axis))
+    return jnp.concatenate(lax.all_to_all(sent, axis, 0, 0), axis=dim)
 
 
 def rms_scale(values, gain_vec):
@@ -64,7 +69,7 @@
         lax.all_gather(up_weight, "fs", axis=0, tiled=True),
         lax.all_gather(pool_weight, "fs", axis=0, tiled=True),
     )
-    down_full = lax.all_gather(down_weight, "fs", axis=1, tiled=True)
+    down_full = swapped_in(down_weight, "fs", 1)
     pool_full = lax.all_gather(pool_half, "tp", axis=2, tiled=True)
     seq_len = tokens.shape[0]
     first_normed = rms_scale(tokens, gain_first)

time: 469 us -> 469 us (level)
  waiting for transfers between devices: 379 us -> 369 us
  starting transfers between devices: 0.38 us -> 6.78 us
    all_gather x1 -> x0, waiting for transfers between devices: 98 us -> none  [shards(): down_full = lax.all_gather(down_weight, 'fs', axis=1, tiled=True)]
    all_gather x1, waiting for transfers between devices: 101 us -> 187 us  [shards(): lax.all_gather(gate_weight, 'fs', axis=0, tiled=True)]
    all_to_all x0 -> x1, starting transfers between devices: none -> 6.48 us  [swapped_in(): return jnp.concatenate(lax.all_to_all(sent, axis, 0, 0), axis=dim)]
  transfers between devices with their start and end apart: 6 -> 6, of which waited for: 6 -> 5; matrix products, arithmetic and copies ran while one was open for 3% -> 3% of each run, Pallas kernels for 0% -> 0%
where the time goes in v1:
time: 469 us; the launch traced here: 468 us
  waiting for transfers between devices  369 us (79%)
  matrix products  45.8 us (10%)
  blocking collectives  16.6 us (4%)
  between operations  13.3 us (3%)
  other arithmetic  11.8 us (3%)
  starting transfers between devices  6.78 us (1%)
    all_gather x1, waiting for transfers between devices, shards(): lax.all_gather(gate_weight, 'fs', axis=0, tiled=True)  187 us
    all_gather x1, waiting for transfers between devices, shards(): lax.all_gather(up_weight, 'fs', axis=0, tiled=True)  94.4 us
    psum x1, waiting for transfers between devices, shards(): lax.psum(jnp.dot(second_hidden, second_down, preferred_element_type=jnp.f...  43 us
    psum x1, waiting for transfers between devices, shards(): lax.psum(jnp.dot(first_hidden, down_full, preferred_element_type=jnp.floa...  24.2 us
    all_gather x1, waiting for transfers between devices, shards(): pool_full = lax.all_gather(pool_half, 'tp', axis=2, tiled=True)  19.1 us
    all_gather x1, blocking collectives, shards(): lax.all_gather(pool_weight, 'fs', axis=0, tiled=True)  16.6 us
    dot_general x2, matrix products, ffn_hidden(): gate_proj = jnp.dot(normed, gate_full, preferred_element_type=jnp.float32)  12 us
    dot_general x4, matrix products, pool_block(): jnp.dot(deviation, pool_full[:, group_number, :], preferred_element_type=...  11.9 us
  transfers between devices with their start and end apart: 6, of which 5 were waited for; matrix products, arithmetic and copies ran while one was open for 3% of the time, Pallas kernels for 0%

profile of v1, /device:TPU:0, one launch (start us, length us, event | category | flops | bytes accessed | tf_op | source)
XLA Modules:
  0.0 468.2 jit_solution(13263021402348207091)
XLA Ops:
  6.5 0.7 all-gather.4.cloned.1.call-update
  7.3 0.7 all-gather.6.cloned.1.call-update
  8.0 0.6 copy.11
  8.6 2.6 stack.2
  11.2 6.5 %all-to-all-start = ((bf16[4,1280,512]{1,2,0:T(8,128)(2,1)}), bf16[4,1280,512]{1,2,0:T(8,128)(2,1)}, u32[]{:S(2)}, u32[]{:S(2)}) async-start(bf16[4,1280,512]{1,2,0:T(8,128)(2,1)} %stack.2), calls=%async_computation | async-start | bytes 10485760 | tf_op jit(solution)/shard_map/all_to_all | solution.py:13
  18.1 187.2 %all-gather.4.cloned.1.call-done = bf16[2048,1280]{1,0:T(8,128)(2,1)} async-done(((bf16[512,1280]{1,0:T(8,128)(2,1)}), bf16[2048,1280]{1,0:T(8,128)(2,1)}) %all-gather.4.cloned.1.call-update) | async-done | bytes 5242896 | tf_op jit(solution)/shard_map/all_gather | solution.py:68
  205.4 6.0 %fusion.56 = f32[384,1280]{1,0:T(8,128)} fusion(bf16[2048,1280]{1,0:T(8,128)(2,1)} %all-gather.4.cloned.1.call-done, bf16[384,2048]{1,0:T(8,128)(2,1)S(1)} %copy-done, f32[2048]{0:T(1024)S(1)} %copy-done.9, f32[384]{0:T(512)S(1)} %add_rsqrt_fusion.2), kind=kOutput, calls=%fused_computation.69 | convolution fusion | flops 2016411648 | bytes 8791552 | tf_op jit(solution)/shard_map/dot_general | solution.py:23
  211.4 94.4 %all-gather.6.cloned.1.call-done = bf16[2048,1280]{1,0:T(8,128)(2,1)} async-done(((bf16[512,1280]{1,0:T(8,128)(2,1)}), bf16[2048,1280]{1,0:T(8,128)(2,1)}) %all-gather.6.cloned.1.call-update) | async-done | bytes 5242896 | tf_op jit(solution)/shard_map/all_gather | solution.py:69
  305.8 10.7 %convolution_convert_fusion.1 = bf16[384,2048]{1,0:T(8,128)(2,1)} fusion(bf16[1280,2048]{0,1:T(8,128)(2,1)} %bitcast.1, bf16[2048,1280]{1,0:T(8,128)(2,1)} %all-gather.6.cloned.1.call-done, f32[384,1280]{1,0:T(8,128)} %fusion.56, bf16[384,2048]{1,0:T(8,128)(2,1)S(1)} %copy-done, f32[2048]{0:T(1024)S(1)} %copy-done.9, f32[384]{0:T(512)S(1)} %add_rsqrt_fusion.2), kind=kOutput, calls=%fused_computation.25 | convolution fusion | flops 4033413120 | bytes 15607296 | tf_op jit(solution)/shard_map/dot_general | solution.py:79
  316.6 16.6 %all_gather.14 = bf16[512,4,128]{2,0,1:T(8,128)(2,1)} all-gather(bf16[128,4,128]{2,0,1:T(8,128)(2,1)S(1)} %copy.12), channel_id=1, replica_groups=mesh['grp'=2,'fs'=4,'tp'=4] {'fs'}, dimensions={0}, use_global_device_ids=true | all-gather | bytes 655360 | tf_op jit(solution)/shard_map/all_gather | solution.py:70
  333.6 24.2 %all-reduce.4.cloned.1.call-done = bf16[384,2048]{1,0:T(8,128)(2,1)} async-done(((bf16[384,2048]{1,0:T(8,128)(2,1)}), bf16[384,2048]{1,0:T(8,128)(2,1)}) %all-reduce.4.cloned.1.call-update) | async-done | bytes 1572880 | tf_op jit(solution)/shard_map/psum | solution.py:78
  357.8 2.2 fusion.4
  360.1 3.0 fusion.97
  363.1 19.1 %all-gather.8.cloned.1.call-done = bf16[512,4,512]{2,0,1:T(8,128)(2,1)} async-done(((bf16[512,4,128]{2,0,1:T(8,128)(2,1)}), bf16[512,4,512]{2,0,1:T(8,128)(2,1)}) %all-gather.8.cloned.1.call-update) | async-done | bytes 2097168 | tf_op jit(solution)/shard_map/all_gather | solution.py:73
  382.2 3.0 convolution_add_fusion
  385.1 3.0 convolution_add_fusion.1
  388.1 3.0 convolution_add_fusion.2
  391.1 3.0 convolution_add_fusion.3
  394.1 2.9 fusion.8
  397.0 1.1 copy-done.2
  398.2 6.0 %fusion.52 = f32[384,1280]{1,0:T(8,128)} fusion(bf16[2048,1280]{1,0:T(8,128)(2,1)} %all-gather.4.cloned.1.call-done, bf16[384,2048]{1,0:T(8,128)(2,1)S(1)} %get-tuple-element.6, f32[2048]{0:T(1024)S(1)} %copy-done.10, f32[384]{0:T(512)S(1)} %add_rsqrt_fusion), kind=kOutput, calls=%fused_computation.68 | convolution fusion | flops 2016411648 | bytes 8791552 | tf_op jit(solution)/shard_map/dot_general | solution.py:23
  404.2 11.2 %convolution_convert_fusion = bf16[384,2048]{1,0:T(8,128)(2,1)} fusion(bf16[1280,2048]{0,1:T(8,128)(2,1)} %bitcast.1, bf16[2048,1280]{1,0:T(8,128)(2,1)} %all-gather.6.cloned.1.call-done, f32[384,1280]{1,0:T(8,128)} %fusion.52, bf16[384,2048]{1,0:T(8,128)(2,1)} %copy-done.2, f32[2048]{0:T(1024)S(1)} %copy-done.10, f32[384]{0:T(512)S(1)} %add_rsqrt_fusion), kind=kOutput, calls=%fused_computation.24 | convolution fusion | flops 4033413120 | bytes 15607296 | tf_op jit(solution)/shard_map/dot_general | solution.py:90
  415.4 43.0 %all-reduce.6.cloned.1.call-done = bf16[384,2048]{1,0:T(8,128)(2,1)} async-done(((bf16[384,2048]{1,0:T(8,128)(2,1)}), bf16[384,2048]{1,0:T(8,128)(2,1)}) %all-reduce.6.cloned.1.call-update) | async-done | bytes 1572880 | tf_op jit(solution)/shard_map/psum | solution.py:89
  458.4 3.2 fusion.11
  (45 shorter events, 0.9 us)
Async XLA Ops:
  6.5 1.5 copy-start.4
  6.5 198.8 %all-gather.4.cloned.1.call-start = ((), (), s32[]{:S(2)}) async-start(), calls=%async_computation.1 | async-start | bytes 6553600 | tf_op jit(solution)/shard_map/all_gather | solution.py:68
  7.3 298.5 %all-gather.6.cloned.1.call-start = ((), (), s32[]{:S(2)}) async-start(), calls=%async_computation.2 | async-start | bytes 6553600 | tf_op jit(solution)/shard_map/all_gather | solution.py:69
  11.2 6.5 %copy-start = (bf16[384,2048]{1,0:T(8,128)(2,1)S(1)}, bf16[384,2048]{1,0:T(8,128)(2,1)}, u32[]{:S(2)}) copy-start(bf16[384,2048]{1,0:T(8,128)(2,1)} %param.10) | copy-start | bytes 4718596
  11.2 194.1 %copy-start.9 = (f32[2048]{0:T(1024)S(1)}, f32[2048]{0:T(1024)}, u32[]{:S(2)}) copy-start(f32[2048]{0:T(1024)} %param.17) | copy-start | bytes 24580
  11.2 294.6 %all-to-all-start = ((bf16[4,1280,512]{1,2,0:T(8,128)(2,1)}), bf16[4,1280,512]{1,2,0:T(8,128)(2,1)}, u32[]{:S(2)}, u32[]{:S(2)}) async-start(bf16[4,1280,512]{1,2,0:T(8,128)(2,1)} %stack.2), calls=%async_computation | async-start | bytes 10485760 | tf_op jit(solution)/shard_map/all_to_all | solution.py:13
  17.7 340.1 %all-reduce.4.cloned.1.call-start = ((), (), s32[]{:S(2)}) async-start(), calls=%async_computation.3 | async-start | bytes 3145728 | tf_op jit(solution)/shard_map/psum | solution.py:78
  305.8 10.8 %copy-start.5 = (bf16[128,4,128]{2,1,0:T(4,128)(2,1)S(1)}, bf16[128,4,128]{2,1,0:T(4,128)(2,1)}, u32[]{:S(2)}) copy-start(bf16[128,4,128]{2,1,0:T(4,128)(2,1)} %param.14) | copy-start | bytes 393220
  305.8 27.8 %copy-start.8 = (f32[4,512]{1,0:T(4,128)S(1)}, f32[4,512]{1,0:T(4,128)}, u32[]{:S(2)}) copy-start(f32[4,512]{1,0:T(4,128)} %param.15) | copy-start | bytes 24580
  316.5 43.6 %copy-start.6 = (f32[2048]{0:T(1024)S(1)}, f32[2048]{0:T(1024)}, u32[]{:S(2)}) copy-start(f32[2048]{0:T(1024)} %param.18) | copy-start | bytes 24580
  316.5 65.7 %all-gather.8.cloned.1.call-start = ((), (), s32[]{:S(2)}) async-start(), calls=%async_computation.4 | async-start | bytes 2621440 | tf_op jit(solution)/shard_map/all_gather | solution.py:73
  333.3 125.1 %all-reduce.6.cloned.1.call-start = ((), (), s32[]{:S(2)}) async-start(), calls=%async_computation.5 | async-start | bytes 3145728 | tf_op jit(solution)/shard_map/psum | solution.py:89
  357.8 2.2 copy-start.1
  391.1 3.0 copy-start.7
  394.1 4.1 copy-start.10
  397.0 1.1 copy-start.2
  404.2 54.2 %copy-start.3 = (bf16[384,2048]{1,0:T(8,128)(2,1)S(1)}, bf16[384,2048]{1,0:T(8,128)(2,1)}, u32[]{:S(2)}) copy-start(bf16[384,2048]{1,0:T(8,128)(2,1)} %copy-done.2) | copy-start | bytes 4718596
Sparse Core Ops, SparseCore 0:
  8.9 196.4 all-gather.3
  206.9 98.8 all-gather.5
  316.6 41.1 all-reduce.3
  359.3 22.8 all-gather.7
  415.5 42.8 all-reduce.5
